TPU v7x, 512 devices: a whole 4x8x8 slice. The times are simulated.
512 devices in a mesh: fs: 64 (over z, y), tp: 8 (over x, core).
Axes of the slice: x: 4, y: 8, z: 8, core: 2. Of those that a mesh axis runs over, the one named last changes fastest.
Arguments:
- tokens: bfloat16 [24576, 2048], P('fs', 'tp'), may hold values from -24 to 24, as said below
- mixer_gain: float32 [2048], replicated, may hold values from 0.1 to 1.9
- w_content: float32 [2048, 1024], P('fs', 'tp'), may hold values from -0.125 to 0.125
- w_spatial: float32 [2048, 1024], P('fs', 'tp'), may hold values from -0.125 to 0.125
- content_scale: float32 [1024], P('tp'), may hold values from 0.5 to 2
- spatial_scale: float32 [1024], P('tp'), may hold values from 0.2 to 3.5, as said below
- spatial_gain: float32 [1024], P('tp'), may hold values from 0.1 to 1.9
- block_mixing: bfloat16 [8, 128, 128], P('tp'), may hold values from -0.5 to 0.5
- block_bias: float32 [8, 128], P('tp'), may hold values from -6 to 6
- w_project: float32 [1024, 2048], P('tp', 'fs'), may hold values from -0.1875 to 0.1875
- project_scale: float32 [2048], P('fs'), may hold values from 0.5 to 2
- channel_gain: float32 [2048], replicated, may hold values from 0.1 to 1.9
- w_up: float32 [2048, 8192], P('fs', 'tp'), may hold values from -0.125 to 0.125
- up_scale: float32 [8192], P('tp'), may hold values from 0.5 to 2
- w_down: float32 [8192, 2048], P('tp', 'fs'), may hold values from -0.0625 to 0.0625
- down_scale: float32 [2048], P('fs'), may hold values from 0.5 to 2
Outputs:
- layer_out: bfloat16 [24576, 2048], P('fs', 'tp')
Inputs may be any that keep to these rules, and one draw needn't show every extreme that they name: `tokens`: activations whose features and rows have differing scales. `spatial_scale`: positive column scales.
All inputs are finite; a program needn't handle non-finite values.
Results may differ from a plain program's by a relative error of at most 0.019.
Values may be sent and summed in bfloat16 or wider, within the bound.
A program may use at most 64 MiB of HBM per device.

v0:
```python
import jax
import jax.numpy as jnp
from jax import lax
from jax.sharding import PartitionSpec as P

EPSILON = 1e-06


def gather_turned(arrays, axis, dims):
    turned = [jnp.moveaxis(a, dim, 0) for a, dim in zip(arrays, dims)]
    both = jnp.concatenate([t.reshape(len(t), -1) for t in turned], axis=1)
    result, at, finished = (lax.all_gather(both, axis, axis=0, tiled=True), 0, [])
    for t, dim in zip(turned, dims):
        section = result[:, at : at + t[0].size].reshape(-1, *t.shape[1:])
        finished.append(jnp.moveaxis(section, 0, dim))
        at += t[0].size
    return tuple(finished)


def in_order(blocks, dim):
    blocks = jnp.moveaxis(blocks, 0, dim)
    dims = blocks.shape
    return blocks.reshape(*dims[:dim], dims[dim] * dims[dim + 1], *dims[dim + 2 :])


def sent_to_all(shard, axis):
    size = lax.axis_size(axis)
    return lax.all_to_all(
        jnp.broadcast_to(shard[None], (size, *shard.shape)), axis, 0, 0, tiled=True
    )


def gathered_copies(shard, axis, dim):
    return in_order(sent_to_all(shard, axis), dim)


def over_copies(shard, axis):
    return sent_to_all(shard, axis).sum(axis=0)


def in_blocks(shard, dim, size):
    before, after = (shard.shape[:dim], shard.shape[dim + 1 :])
    return jnp.moveaxis(shard.reshape(*before, size, -1, *after), dim, 0)


def summed_on_arrival(shard, axis, dim):
    size = lax.axis_size(axis)
    blocks = lax.all_to_all(in_blocks(shard, dim, size), axis, 0, 0, tiled=True)
    return jnp.sum(blocks.astype(jnp.float32), axis=0)


def normalize_rows(token_rows, gain_vector):
    values = token_rows.astype(jnp.float32)
    scaled = values * lax.rsqrt(jnp.mean(values * values, axis=-1, keepdims=True) + EPSILON)
    return (scaled * gain_vector).astype(jnp.bfloat16)


def shards(
    tokens,
    mixer_gain,
    w_content,
    w_spatial,
    content_scale,
    spatial_scale,
    spatial_gain,
    block_mixing,
    block_bias,
    w_project,
    project_scale,
    channel_gain,
    w_up,
    up_scale,
    w_down,
    down_scale,
):
    content_weight = w_content.astype(jnp.bfloat16)
    spatial_weight = w_spatial.astype(jnp.bfloat16)
    project_weight = w_project.astype(jnp.bfloat16)
    up_weight = w_up.astype(jnp.bfloat16)
    down_weight = w_down.astype(jnp.bfloat16)
    project_full, down_full = gather_turned((project_scale, down_scale), "fs", (0, 0))
    gathered_rows = gathered_copies(tokens, "tp", 1)
    normed = normalize_rows(gathered_rows, mixer_gain)
    row_count = gathered_rows.shape[0]
    content_full, spatial_full, project_cols = gather_turned(
        (content_weight, spatial_weight, project_weight), "fs", (0, 0, 1)
    )
    content_linear = jnp.dot(normed, content_full, preferred_element_type=jnp.float32)
    spatial_linear = jnp.dot(normed, spatial_full, preferred_element_type=jnp.float32)
    content = jax.nn.gelu(content_linear * content_scale)
    spatial = jax.nn.gelu(spatial_linear * spatial_scale)
    square_sums = over_copies(jnp.sum(spatial * spatial, axis=1), "tp")
    total_width = spatial.shape[1] * lax.axis_size("tp")
    spatial_norm = (
        spatial * lax.rsqrt(square_sums / total_width + EPSILON)[:, None] * spatial_gain
    ).astype(jnp.bfloat16)
    groups_here = block_mixing.shape[0]
    block_size = block_mixing.shape[1]
    group_width = spatial_norm.shape[1] // groups_here
    causal_mask = jnp.tril(jnp.ones((block_size, block_size), dtype=bool))
    mixing_weights = jnp.where(causal_mask[None, :, :], block_mixing, jnp.zeros_like(block_mixing))
    grouped = spatial_norm.reshape(row_count // block_size, block_size, groups_here, group_width)
    mixed_block = (
        jnp.einsum("gts,nsgc->ntgc", mixing_weights, grouped, preferred_element_type=jnp.float32)
        + block_bias.T[None, :, :, None]
    )
    gated = (content * mixed_block.reshape(row_count, spatial_norm.shape[1])).astype(jnp.bfloat16)
    mixer_terms = jnp.dot(gated, project_cols, preferred_element_type=jnp.float32) * project_full
    mixer_sum = summed_on_arrival(mixer_terms.astype(jnp.bfloat16), "tp", 1)
    middle = (tokens.astype(jnp.float32) + mixer_sum).astype(jnp.bfloat16)
    middle_rows = gathered_copies(middle, "tp", 1)
    channel_normed = normalize_rows(middle_rows, channel_gain)
    up_full, down_cols = gather_turned((up_weight, down_weight), "fs", (0, 1))
    up_linear = jnp.dot(channel_normed, up_full, preferred_element_type=jnp.float32)
    hidden = jnp.square(jax.nn.relu(up_linear * up_scale)).astype(jnp.bfloat16)
    channel_terms = jnp.dot(hidden, down_cols, preferred_element_type=jnp.float32) * down_full
    channel_sum = summed_on_arrival(channel_terms.astype(jnp.bfloat16), "tp", 1)
    return (middle.astype(jnp.float32) + channel_sum).astype(jnp.bfloat16)


def solution(mesh):
    return jax.shard_map(
        shards,
        mesh=mesh,
        in_specs=(
            P("fs", "tp"),
            P(),
            P("fs", "tp"),
            P("fs", "tp"),
            P("tp"),
            P("tp"),
            P("tp"),
            P("tp", None, None),
            P("tp", None),
            P("tp", "fs"),
            P("fs"),
            P(),
            P("fs", "tp"),
            P("tp"),
            P("tp", "fs"),
            P("fs"),
        ),
        out_specs=P("fs", "tp"),
        check_vma=False,
    )
```

profile of v0, /device:TPU:1, one launch (start us, length us, event | category | flops | bytes accessed | tf_op | source)
XLA Modules:
  0.0 238.0 jit_solution(6624533297289008726)
XLA Ops:
  6.5 0.0 all-gather.4.cloned.1.call-start
  6.5 0.7 convert_bitcast_fusion.1
  7.3 0.7 convert_element_type.86
  8.0 0.7 convert_element_type.87
  8.7 0.6 pad_maximum_fusion.1
  9.3 0.0 all-gather.4.cloned.1.call-update
  9.3 0.0 all-gather.6.cloned.1.call-start
  9.4 0.9 convert_element_type.100
  10.3 0.9 convert_bitcast_fusion
  11.2 0.7 pad_maximum_fusion
  11.9 0.0 all-gather.6.cloned.1.call-update
  11.9 1.1 copy.30
  13.0 1.3 broadcast_in_dim.9
  14.3 0.0 copy-start.6
  14.3 0.0 copy-start.7
  14.3 10.5 %all-to-all-start = ((bf16[8,384,256]{1,2,0:T(8,128)(2,1)}), bf16[8,384,256]{1,2,0:T(8,128)(2,1)S(1)}, u32[]{:S(2)}, u32[]{:S(2)}) async-start(bf16[8,384,256]{1,2,0:T(8,128)(2,1)} %broadcast_in_dim.9), calls=%async_computation | async-start | bytes 3145728 | tf_op jit(solution)/shard_map/all_to_all | solution.py:28
  24.7 0.0 copy-start.2
  24.7 0.0 copy-done.6
  24.7 0.0 copy-done.7
  24.8 42.5 %all-gather = f32[64,32,2]{1,2,0:T(2,128)S(1)} all-gather(f32[1,32,2]{1,2,0:T(2,128)S(1)} %maximum_bitcast_fusion), channel_id=1, replica_groups=mesh['fs'=64,'tp'=8] {'fs'}, dimensions={0}, use_global_device_ids=true | all-gather | bytes 16640 | tf_op jit(solution)/shard_map/all_gather | solution.py:12
  67.3 0.1 reshape.91
  67.4 0.0 all-to-all-done
  67.4 0.4 multiply_reduce_fusion.1
  67.8 0.0 copy-done.2
  67.8 0.0 copy-start.9
  67.9 0.4 fusion.7
  68.3 0.0 copy-start.4
  68.3 0.0 copy-start.1
  68.3 0.0 copy-start.5
  68.3 0.0 copy-start.10
  68.3 25.8 %all-gather.4.cloned.1.call-done = bf16[2048,384]{1,0:T(8,128)(2,1)} async-done(((bf16[32,384]{1,0:T(8,128)(2,1)}), bf16[2048,384]{1,0:T(8,128)(2,1)}) %all-gather.4.cloned.1.call-update) | async-done | bytes 1572880 | tf_op jit(solution)/shard_map/all_gather | solution.py:12
  94.1 0.0 copy-done.9
  94.1 1.8 multiply_reduce_fusion.2
  95.8 0.6 broadcast_in_dim.10
  96.5 9.5 %all-to-all-start.1 = ((f32[8,1,384]{2,1,0:T(1,128)}), f32[8,1,384]{2,1,0:T(1,128)S(1)}, u32[]{:S(2)}, u32[]{:S(2)}) async-start(f32[8,1,384]{2,1,0:T(1,128)} %broadcast_in_dim.10), calls=%async_computation.1 | async-start | bytes 24576 | tf_op jit(solution)/shard_map/all_to_all | solution.py:28
  106.0 4.6 %all-to-all-done.1 = f32[8,1,384]{2,1,0:T(1,128)S(1)} async-done(((f32[8,1,384]{2,1,0:T(1,128)}), f32[8,1,384]{2,1,0:T(1,128)S(1)}, u32[]{:S(2)}, u32[]{:S(2)}) %all-to-all-start.1) | async-done | bytes 12320 | tf_op jit(solution)/shard_map/all_to_all | solution.py:28
  110.7 0.0 copy-done.4
  110.7 0.1 multiply_convert_fusion.3
  110.8 0.0 copy-done.1
  110.8 0.0 copy-done.5
  110.8 0.2 fusion.14
  111.0 0.0 copy-done.10
  111.0 3.0 %multiply_convert_fusion.1 = bf16[384,2048]{1,0:T(8,128)(2,1)S(1)} fusion(f32[2048]{0:T(1024)S(1)} %bitcast.66, bf16[2048,384]{1,0:T(8,128)(2,1)} %all-gather.4.cloned.1.call-done, f32[384,128]{1,0:T(8,128)S(1)} %bitcast.64, bf16[384,2048]{0,1:T(8,128)(2,1)S(1)} %fusion.7, f32[128]{0:T(128)S(1)} %copy-done.10), kind=kOutput, calls=%fused_computation.14 | convolution fusion | flops 404766720 | bytes 4399616 | tf_op jit(solution)/shard_map/dot_general | solution.py:108
  114.0 0.1 copy.42
  114.2 23.7 %all_to_all.26 = bf16[8,384,256]{2,1,0:T(8,128)(2,1)S(1)} all-to-all(bf16[8,384,256]{2,1,0:T(8,128)(2,1)S(1)} %bitcast.59), channel_id=1, replica_groups=mesh['fs'=64,'tp'=8] {'tp'}, dimensions={0} | all-to-all | bytes 3145728 | tf_op jit(solution)/shard_map/all_to_all | solution.py:48
  137.8 0.0 copy-start
  137.8 0.2 convert_reduce_fusion.1
  138.1 0.7 copy-done
  138.8 0.2 copy.34
  139.0 0.1 broadcast_in_dim.12
  139.1 24.1 %all_to_all.27 = bf16[8,384,256]{1,2,0:T(8,128)(2,1)S(1)} all-to-all(bf16[8,384,256]{1,2,0:T(8,128)(2,1)S(1)} %broadcast_in_dim.12), channel_id=1, replica_groups=mesh['fs'=64,'tp'=8] {'tp'}, dimensions={0} | all-to-all | bytes 3145728 | tf_op jit(solution)/shard_map/all_to_all | solution.py:28
  163.2 0.0 copy-start.3
  163.2 0.4 multiply_reduce_fusion
  163.6 0.3 copy-done.3
  163.9 0.0 copy-start.8
  163.9 0.4 fusion.5
  164.3 33.2 %all-gather.6.cloned.1.call-done = bf16[2048,2048]{1,0:T(8,128)(2,1)} async-done(((bf16[32,2048]{1,0:T(8,128)(2,1)}), bf16[2048,2048]{1,0:T(8,128)(2,1)}) %all-gather.6.cloned.1.call-update) | async-done | bytes 8388624 | tf_op jit(solution)/shard_map/all_gather | solution.py:12
  197.6 0.0 copy-done.8
  197.6 6.9 %multiply_convert_fusion = bf16[384,2048]{1,0:T(8,128)(2,1)S(1)} fusion(bf16[2048,2048]{1,0:T(8,128)(2,1)} %all-gather.6.cloned.1.call-done, f32[2048]{0:T(1024)S(1)} %bitcast.65, bf16[384,2048]{0,1:T(8,128)(2,1)S(1)} %fusion.5, f32[1024]{0:T(1024)S(1)} %copy-done.8), kind=kOutput, calls=%fused_computation.11 | convolution fusion | flops 3224371200 | bytes 11546624 | tf_op jit(solution)/shard_map/dot_general | solution.py:116
  204.5 0.1 copy.41
  204.6 25.5 %all_to_all.28 = bf16[8,384,256]{2,1,0:T(8,128)(2,1)S(1)} all-to-all(bf16[8,384,256]{2,1,0:T(8,128)(2,1)S(1)} %bitcast.60), channel_id=1, replica_groups=mesh['fs'=64,'tp'=8] {'tp'}, dimensions={0} | all-to-all | bytes 3145728 | tf_op jit(solution)/shard_map/all_to_all | solution.py:48
  230.2 0.2 convert_reduce_fusion
  230.4 0.7 add_convert_fusion
  (8 shorter events, 0.1 us)
Async XLA Ops:
  6.5 87.6 %all-gather.4.cloned.1.call-start = ((), (), s32[]{:S(2)}) async-start(), calls=%async_computation.5 | async-start | bytes 1597440 | tf_op jit(solution)/shard_map/all_gather | solution.py:12
  9.3 188.2 %all-gather.6.cloned.1.call-start = ((), (), s32[]{:S(2)}) async-start(), calls=%async_computation.6 | async-start | bytes 8519680 | tf_op jit(solution)/shard_map/all_gather | solution.py:12
  14.3 10.5 %copy-start.6 = (f32[32]{0:T(128)S(1)}, f32[32]{0:T(128)}, u32[]{:S(2)}) copy-start(f32[32]{0:T(128)} %param.31) | copy-start | bytes 388
  14.3 10.5 %copy-start.7 = (f32[32]{0:T(128)S(1)}, f32[32]{0:T(128)}, u32[]{:S(2)}) copy-start(f32[32]{0:T(128)} %param.26) | copy-start | bytes 388
  14.3 53.1 %all-to-all-start = ((bf16[8,384,256]{1,2,0:T(8,128)(2,1)}), bf16[8,384,256]{1,2,0:T(8,128)(2,1)S(1)}, u32[]{:S(2)}, u32[]{:S(2)}) async-start(bf16[8,384,256]{1,2,0:T(8,128)(2,1)} %broadcast_in_dim.9), calls=%async_computation | async-start | bytes 3145728 | tf_op jit(solution)/shard_map/all_to_all | solution.py:28
  24.7 43.1 %copy-start.2 = (f32[2048]{0:T(1024)S(1)}, f32[2048]{0:T(1024)}, u32[]{:S(2)}) copy-start(f32[2048]{0:T(1024)} %param.17) | copy-start | bytes 24580
  67.8 26.2 %copy-start.9 = (f32[128]{0:T(128)S(1)}, f32[128]{0:T(128)}, u32[]{:S(2)}) copy-start(f32[128]{0:T(128)} %param.21) | copy-start | bytes 1540
  68.3 42.4 %copy-start.4 = (f32[128]{0:T(128)S(1)}, f32[128]{0:T(128)}, u32[]{:S(2)}) copy-start(f32[128]{0:T(128)} %param.22) | copy-start | bytes 1540
  68.3 42.5 %copy-start.1 = (bf16[1,128,128]{2,1,0:T(8,128)(2,1)S(1)}, bf16[1,128,128]{2,1,0:T(8,128)(2,1)}, u32[]{:S(2)}) copy-start(bf16[1,128,128]{2,1,0:T(8,128)(2,1)} %param.23) | copy-start | bytes 98308
  68.3 42.5 %copy-start.5 = (f32[1,128]{1,0:T(1,128)S(1)}, f32[1,128]{1,0:T(1,128)}, u32[]{:S(2)}) copy-start(f32[1,128]{1,0:T(1,128)} %param.24) | copy-start | bytes 1540
  68.3 42.7 %copy-start.10 = (f32[128]{0:T(128)S(1)}, f32[128]{0:T(128)}, u32[]{:S(2)}) copy-start(f32[128]{0:T(128)} %param.20) | copy-start | bytes 1540
  96.5 14.2 %all-to-all-start.1 = ((f32[8,1,384]{2,1,0:T(1,128)}), f32[8,1,384]{2,1,0:T(1,128)S(1)}, u32[]{:S(2)}, u32[]{:S(2)}) async-start(f32[8,1,384]{2,1,0:T(1,128)} %broadcast_in_dim.10), calls=%async_computation.1 | async-start | bytes 24576 | tf_op jit(solution)/shard_map/all_to_all | solution.py:28
  137.8 0.9 copy-start
  163.2 0.7 copy-start.3
  163.9 33.7 %copy-start.8 = (f32[1024]{0:T(1024)S(1)}, f32[1024]{0:T(1024)}, u32[]{:S(2)}) copy-start(f32[1024]{0:T(1024)} %param.29) | copy-start | bytes 12292
Sparse Core Ops, SparseCore 0:
  10.3 83.7 all-gather.3
  97.1 100.3 all-gather.5
where the time goes:
time: 239 us; the launch traced here: 238 us
  blocking collectives  116 us (49%)
  waiting for transfers between devices  63.6 us (27%)
  starting transfers between devices  20 us (8%)
  between operations  13.6 us (6%)
  matrix products  11.9 us (5%)
  other arithmetic  8.33 us (3%)
  local copies, waits for them, and re-layouts  4.63 us (2%)
    all_gather x2, waiting for transfers between devices, gather_turned(): lax.all_gather(both, axis, axis=0, tiled=True)  59 us
    all_to_all x2, blocking collectives, summed_on_arrival(): blocks = lax.all_to_all(in_blocks(shard, dim, size), axis, 0, 0, tiled=True)  49.2 us
    all_gather x1, blocking collectives, gather_turned(): lax.all_gather(both, axis, axis=0, tiled=True)  42.5 us
    all_to_all x1, blocking collectives, sent_to_all(): lax.all_to_all(jnp.broadcast_to(shard[None], (size, *shard.shape)), axis,...  24.1 us
    all_to_all x2, starting transfers between devices, sent_to_all(): lax.all_to_all(jnp.broadcast_to(shard[None], (size, *shard.shape)), axis,...  20 us
    dot_general x1, matrix products, shards(): jnp.dot(hidden, down_cols, preferred_element_type=jnp.float32) * down_full  6.94 us
  transfers between devices with their start and end apart: 4, of which 3 were waited for; matrix products, arithmetic and copies ran while one was open for 5% of the time, Pallas kernels for 0%

commit v1 on v0

--- a/solution.py
+++ b/solution.py
@@ -9,7 +9,13 @@
 def gather_turned(arrays, axis, dims):
     turned = [jnp.moveaxis(a, dim, 0) for a, dim in zip(arrays, dims)]
     both = jnp.concatenate([t.reshape(len(t), -1) for t in turned], axis=1)
-    result, at, finished = (lax.all_gather(both, axis, axis=0, tiled=True), 0, [])
+    result, at, finished = (
+        jnp.concatenate(
+            lax.all_to_all(jnp.stack([both] * lax.axis_size(axis)), axis, 0, 0), axis=0
+        ),
+        0,
+        [],
+    )
     for t, dim in zip(turned, dims):
         section = result[:, at : at + t[0].size].reshape(-1, *t.shape[1:])
         finished.append(jnp.moveaxis(section, 0, dim))

time: 239 us -> 503 us (2.10)
  the two profiles are of different devices: /device:TPU:1 before, /device:TPU:40 now
where the time goes in v1:
time: 503 us
  waiting for transfers between devices  356 us (71%)
  blocking collectives  69.7 us (14%)
  starting transfers between devices  47.1 us (9%)
  matrix products  12.5 us (2%)
  local copies, waits for them, and re-layouts  12.2 us (2%)
    all_to_all x3, waiting for transfers between devices, gather_turned(): lax.all_to_all(jnp.stack([both] * lax.axis_size(axis)), axis, 0, 0)  308 us
    all_to_all x2, blocking collectives, summed_on_arrival(): blocks = lax.all_to_all(in_blocks(shard, dim, size), axis, 0, 0, tiled=True)  69.7 us
    all_to_all x3, waiting for transfers between devices, sent_to_all(): lax.all_to_all(jnp.broadcast_to(shard[None], (size, *shard.shape)), axis,...  48.1 us
    all_to_all x3, starting transfers between devices, gather_turned(): lax.all_to_all(jnp.stack([both] * lax.axis_size(axis)), axis, 0, 0)  35.6 us
    all_to_all x3, starting transfers between devices, sent_to_all(): lax.all_to_all(jnp.broadcast_to(shard[None], (size, *shard.shape)), axis,...  11.5 us
  transfers between devices with their start and end apart: 6, of which 6 were waited for; matrix products, arithmetic and copies ran while one was open for 1% of the time, Pallas kernels for 0%

profile of v1, /device:TPU:40, one launch (start us, length us, event | category | flops | bytes accessed | tf_op | source)
XLA Modules:
  0.0 502.6 jit_solution(14537414184500478883)
XLA Ops:
  0.0 0.7 pad_maximum_fusion.2
  0.7 0.6 stack.7
  1.3 16.1 %all-to-all-start.3 = ((f32[64,32,2]{1,2,0:T(2,128)}), f32[64,32,2]{1,2,0:T(2,128)S(1)}, u32[]{:S(2)}, u32[]{:S(2)}) async-start(f32[64,32,2]{1,2,0:T(2,128)} %stack.7), calls=%async_computation.3 | async-start | bytes 131072 | tf_op jit(solution)/shard_map/all_to_all | solution.py:14
  17.5 1.1 copy.32
  18.6 6.9 %all-to-all-done.3 = f32[64,32,2]{1,2,0:T(2,128)S(1)} async-done(((f32[64,32,2]{1,2,0:T(2,128)}), f32[64,32,2]{1,2,0:T(2,128)S(1)}, u32[]{:S(2)}, u32[]{:S(2)}) %all-to-all-start.3) | async-done | bytes 16416 | tf_op jit(solution)/shard_map/all_to_all | solution.py:14
  25.4 1.3 broadcast_in_dim.9
  26.7 0.0 copy-start.4
  26.7 0.0 copy-start.5
  26.7 0.0 copy-start.6
  26.7 4.4 all-to-all-start
  31.2 0.0 copy-done.4
  31.2 0.0 copy-done.5
  31.2 0.0 copy-done.6
  31.2 21.5 %all-to-all-done = bf16[8,384,256]{1,2,0:T(8,128)(2,1)S(1)} async-done(((bf16[8,384,256]{1,2,0:T(8,128)(2,1)}), bf16[8,384,256]{1,2,0:T(8,128)(2,1)S(1)}, u32[]{:S(2)}, u32[]{:S(2)}) %all-to-all-start) | async-done | bytes 1572896 | tf_op jit(solution)/shard_map/all_to_all | solution.py:34
  52.7 1.3 stack.6
  54.0 8.8 %all-to-all-start.1 = ((bf16[64,32,384]{2,1,0:T(8,128)(2,1)}), bf16[64,32,384]{2,1,0:T(8,128)(2,1)S(1)}, u32[]{:S(2)}, u32[]{:S(2)}) async-start(bf16[64,32,384]{2,1,0:T(8,128)(2,1)} %stack.6), calls=%async_computation.1 | async-start | bytes 3145728 | tf_op jit(solution)/shard_map/all_to_all | solution.py:14
  62.9 0.0 copy-start.7
  62.9 0.1 reshape.102
  63.0 0.4 multiply_reduce_fusion.1
  63.4 0.2 copy-done.7
  63.6 0.0 copy-start.12
  63.6 1.6 fusion.7
  65.1 36.3 %all-to-all-done.1 = bf16[64,32,384]{2,1,0:T(8,128)(2,1)S(1)} async-done(((bf16[64,32,384]{2,1,0:T(8,128)(2,1)}), bf16[64,32,384]{2,1,0:T(8,128)(2,1)S(1)}, u32[]{:S(2)}, u32[]{:S(2)}) %all-to-all-start.1) | async-done | bytes 1572896 | tf_op jit(solution)/shard_map/all_to_all | solution.py:14
  101.4 0.0 copy-done.12
  101.4 0.0 copy-start.9
  101.4 0.0 copy-start.3
  101.4 0.0 copy-start.10
  101.4 0.0 copy-start.13
  101.4 2.1 multiply_reduce_fusion.2
  103.6 0.6 broadcast_in_dim.10
  104.2 3.3 all-to-all-start.2
  107.6 5.2 %all-to-all-done.2 = f32[8,1,384]{2,1,0:T(1,128)S(1)} async-done(((f32[8,1,384]{2,1,0:T(1,128)}), f32[8,1,384]{2,1,0:T(1,128)S(1)}, u32[]{:S(2)}, u32[]{:S(2)}) %all-to-all-start.2) | async-done | bytes 12320 | tf_op jit(solution)/shard_map/all_to_all | solution.py:34
  112.8 0.0 copy-done.9
  112.9 0.1 multiply_convert_fusion.3
  113.0 0.0 copy-done.3
  113.0 0.0 copy-done.10
  113.0 0.2 fusion.14
  113.2 0.0 copy-done.13
  113.2 3.2 multiply_convert_fusion.1
  116.4 0.1 copy.44
  116.5 24.0 %all_to_all.41 = bf16[8,384,256]{2,1,0:T(8,128)(2,1)S(1)} all-to-all(bf16[8,384,256]{2,1,0:T(8,128)(2,1)S(1)} %bitcast.59), channel_id=1, replica_groups=mesh['fs'=64,'tp'=8] {'tp'}, dimensions={0} | all-to-all | bytes 3145728 | tf_op jit(solution)/shard_map/all_to_all | solution.py:54
  140.6 0.0 copy-start
  140.6 0.2 convert_reduce_fusion.1
  140.8 0.7 copy-done
  141.5 0.2 copy.36
  141.7 1.3 broadcast_in_dim.12
  143.0 0.0 copy-start.1
  143.0 3.7 all-to-all-start.5
  146.7 0.0 copy-done.1
  146.8 0.0 copy-done.2
  146.8 21.4 %all-to-all-done.5 = bf16[8,384,256]{1,2,0:T(8,128)(2,1)S(1)} async-done(((bf16[8,384,256]{1,2,0:T(8,128)(2,1)}), bf16[8,384,256]{1,2,0:T(8,128)(2,1)S(1)}, u32[]{:S(2)}, u32[]{:S(2)}) %all-to-all-start.5) | async-done | bytes 1572896 | tf_op jit(solution)/shard_map/all_to_all | solution.py:34
  168.2 4.3 stack.8
  172.5 10.6 %all-to-all-start.6 = ((bf16[64,32,2048]{2,1,0:T(8,128)(2,1)}), bf16[64,32,2048]{2,1,0:T(8,128)(2,1)}, u32[]{:S(2)}, u32[]{:S(2)}) async-start(bf16[64,32,2048]{2,1,0:T(8,128)(2,1)} %stack.8), calls=%async_computation.6 | async-start | bytes 16777216 | tf_op jit(solution)/shard_map/all_to_all | solution.py:14
  183.1 0.0 copy-start.8
  183.1 0.4 multiply_reduce_fusion
  183.6 0.3 copy-done.8
  183.8 0.4 fusion.5
  184.2 264.7 %all-to-all-done.6 = bf16[64,32,2048]{2,1,0:T(8,128)(2,1)} async-done(((bf16[64,32,2048]{2,1,0:T(8,128)(2,1)}), bf16[64,32,2048]{2,1,0:T(8,128)(2,1)}, u32[]{:S(2)}, u32[]{:S(2)}) %all-to-all-start.6) | async-done | bytes 8388640 | tf_op jit(solution)/shard_map/all_to_all | solution.py:14
  449.0 0.0 copy-done.11
  449.0 6.9 %multiply_convert_fusion = bf16[384,2048]{1,0:T(8,128)(2,1)S(1)} fusion(bf16[2048,2048]{1,0:T(8,128)(2,1)} %bitcast.18, f32[2048]{0:T(1024)S(1)} %bitcast.67, bf16[384,2048]{0,1:T(8,128)(2,1)S(1)} %fusion.5, f32[1024]{0:T(1024)S(1)} %copy-done.11), kind=kOutput, calls=%fused_computation.11 | convolution fusion | flops 3224371200 | bytes 11546624 | tf_op jit(solution)/shard_map/dot_general | solution.py:122
  455.9 0.1 copy.43
  456.0 45.6 %all_to_all.42 = bf16[8,384,256]{2,1,0:T(8,128)(2,1)S(1)} all-to-all(bf16[8,384,256]{2,1,0:T(8,128)(2,1)S(1)} %bitcast.60), channel_id=1, replica_groups=mesh['fs'=64,'tp'=8] {'tp'}, dimensions={0} | all-to-all | bytes 3145728 | tf_op jit(solution)/shard_map/all_to_all | solution.py:54
  501.6 0.2 convert_reduce_fusion
  501.9 0.7 add_convert_fusion
  (16 shorter events, 0.2 us)
Async XLA Ops:
  1.3 24.1 %all-to-all-start.3 = ((f32[64,32,2]{1,2,0:T(2,128)}), f32[64,32,2]{1,2,0:T(2,128)S(1)}, u32[]{:S(2)}, u32[]{:S(2)}) async-start(f32[64,32,2]{1,2,0:T(2,128)} %stack.7), calls=%async_computation.3 | async-start | bytes 131072 | tf_op jit(solution)/shard_map/all_to_all | solution.py:14
  26.7 4.4 copy-start.4
  26.7 4.5 copy-start.5
  26.7 4.5 copy-start.6
  26.7 26.0 %all-to-all-start = ((bf16[8,384,256]{1,2,0:T(8,128)(2,1)}), bf16[8,384,256]{1,2,0:T(8,128)(2,1)S(1)}, u32[]{:S(2)}, u32[]{:S(2)}) async-start(bf16[8,384,256]{1,2,0:T(8,128)(2,1)} %broadcast_in_dim.9), calls=%async_computation | async-start | bytes 3145728 | tf_op jit(solution)/shard_map/all_to_all | solution.py:34
  54.0 47.4 %all-to-all-start.1 = ((bf16[64,32,384]{2,1,0:T(8,128)(2,1)}), bf16[64,32,384]{2,1,0:T(8,128)(2,1)S(1)}, u32[]{:S(2)}, u32[]{:S(2)}) async-start(bf16[64,32,384]{2,1,0:T(8,128)(2,1)} %stack.6), calls=%async_computation.1 | async-start | bytes 3145728 | tf_op jit(solution)/shard_map/all_to_all | solution.py:14
  62.9 0.7 copy-start.7
  63.6 37.9 %copy-start.12 = (f32[128]{0:T(128)S(1)}, f32[128]{0:T(128)}, u32[]{:S(2)}) copy-start(f32[128]{0:T(128)} %param.21) | copy-start | bytes 1540
  101.4 11.4 %copy-start.9 = (f32[128]{0:T(128)S(1)}, f32[128]{0:T(128)}, u32[]{:S(2)}) copy-start(f32[128]{0:T(128)} %param.22) | copy-start | bytes 1540
  101.4 11.6 %copy-start.3 = (bf16[1,128,128]{2,1,0:T(8,128)(2,1)S(1)}, bf16[1,128,128]{2,1,0:T(8,128)(2,1)}, u32[]{:S(2)}) copy-start(bf16[1,128,128]{2,1,0:T(8,128)(2,1)} %param.23) | copy-start | bytes 98308
  101.4 11.6 %copy-start.10 = (f32[1,128]{1,0:T(1,128)S(1)}, f32[1,128]{1,0:T(1,128)}, u32[]{:S(2)}) copy-start(f32[1,128]{1,0:T(1,128)} %param.24) | copy-start | bytes 1540
  101.4 11.7 %copy-start.13 = (f32[128]{0:T(128)S(1)}, f32[128]{0:T(128)}, u32[]{:S(2)}) copy-start(f32[128]{0:T(128)} %param.20) | copy-start | bytes 1540
  104.2 8.6 %all-to-all-start.2 = ((f32[8,1,384]{2,1,0:T(1,128)}), f32[8,1,384]{2,1,0:T(1,128)S(1)}, u32[]{:S(2)}, u32[]{:S(2)}) async-start(f32[8,1,384]{2,1,0:T(1,128)} %broadcast_in_dim.10), calls=%async_computation.2 | async-start | bytes 24576 | tf_op jit(solution)/shard_map/all_to_all | solution.py:34
  140.6 0.9 copy-start
  143.0 3.7 copy-start.1
  143.0 3.8 copy-start.2
  143.0 25.2 %all-to-all-start.5 = ((bf16[8,384,256]{1,2,0:T(8,128)(2,1)}), bf16[8,384,256]{1,2,0:T(8,128)(2,1)S(1)}, u32[]{:S(2)}, u32[]{:S(2)}) async-start(bf16[8,384,256]{1,2,0:T(8,128)(2,1)} %broadcast_in_dim.12), calls=%async_computation.5 | async-start | bytes 3145728 | tf_op jit(solution)/shard_map/all_to_all | solution.py:34
  172.5 276.5 %all-to-all-start.6 = ((bf16[64,32,2048]{2,1,0:T(8,128)(2,1)}), bf16[64,32,2048]{2,1,0:T(8,128)(2,1)}, u32[]{:S(2)}, u32[]{:S(2)}) async-start(bf16[64,32,2048]{2,1,0:T(8,128)(2,1)} %stack.8), calls=%async_computation.6 | async-start | bytes 16777216 | tf_op jit(solution)/shard_map/all_to_all | solution.py:14
  183.1 0.7 copy-start.8
  183.8 265.2 %copy-start.11 = (f32[1024]{0:T(1024)S(1)}, f32[1024]{0:T(1024)}, u32[]{:S(2)}) copy-start(f32[1024]{0:T(1024)} %param.29) | copy-start | bytes 12292
